TPU v7x, 32 devices: a whole 2x2x4 slice. The times are simulated.
32 devices in a mesh: grp: 2 (over y), kv: 4 (over z), tp: 4 (over x, core).
Axes of the slice: x: 2, y: 2, z: 4, core: 2. Of those that a mesh axis runs over, the one named last changes fastest.
Arguments:
- tokens: bfloat16 [32, 4096], P('grp', 'kv'), parts along dimension 0, may hold values from -40 to 40
- lengths: int32 [32], P(('grp', 'kv')), parts along dimension 0, may hold values from 1 to 6, 40 in all
- conv_state_x: bfloat16 [32, 3, 4096], P(('grp', 'kv'), None, 'tp'), parts along dimension 0, may hold values from -6 to 6
- conv_state_bc: bfloat16 [32, 3, 2, 1024], P(('grp', 'kv'), None, None, 'tp'), parts along dimension 0, may hold values from -6 to 6
- ssm_state: float32 [32, 64, 64, 128], P(('grp', 'kv'), 'tp'), parts along dimension 0, may hold values from -0.6 to 0.6
- norm_gain: bfloat16 [4096], P('kv'), may hold values from 0.099609375 to 1.8984375
- w_gate: bfloat16 [4096, 4096], P('kv', 'tp'), may hold values from -0.09375 to 0.09375
- w_value: bfloat16 [4096, 4096], P('kv', 'tp'), may hold values from -0.09375 to 0.09375
- w_key: bfloat16 [4096, 1024], P('kv', 'tp'), may hold values from -0.09375 to 0.09375
- w_query: bfloat16 [4096, 1024], P('kv', 'tp'), may hold values from -0.09375 to 0.09375
- w_step: bfloat16 [4096, 64], P('kv', 'tp'), may hold values from -0.09375 to 0.09375
- step_bias: float32 [64], P('tp'), may hold values from -2 to 0
- decay_log: float32 [64], P('tp'), may hold values from -2 to 1
- conv_x: bfloat16 [4, 4096], P(None, 'tp'), may hold values from -3 to 3
- conv_bc: bfloat16 [4, 2, 1024], P(None, None, 'tp'), may hold values from -3 to 3
- inner_gain: bfloat16 [4096], P('tp'), may hold values from 0.099609375 to 1.8984375
- w_out: bfloat16 [4096, 4096], P('tp', 'kv'), may hold values from -0.09375 to 0.09375
- mlp_gain: bfloat16 [4096], P('kv'), may hold values from 0.099609375 to 1.8984375
- w_up: bfloat16 [4096, 16384], P('kv', 'tp'), may hold values from -0.09375 to 0.09375
- w_down: bfloat16 [16384, 4096], P('tp', 'kv'), may hold values from -0.046875 to 0.046875
Outputs:
- layer_out: bfloat16 [32, 4096], P('grp', 'kv'), parts along dimension 0
- next_state: float32 [32, 64, 64, 128], P(('grp', 'kv'), 'tp'), parts along dimension 0
There are 2 independent parts, one for each index of `grp`. A program takes and returns all parts, laid end to end along the dimension named above; an argument that names none is the same for every part. Nothing has to cross between parts.
All inputs are finite; a program needn't handle non-finite values. No bound on the sum of `lengths` on one device may be relied on, other than what follows from the above.
Results may differ from a plain program's by a relative error of at most 0.008.
Values may be sent and summed in bfloat16 or wider, within the bound.
A program may use at most 64 MiB of HBM per device.

v0:
```python
import jax
import jax.numpy as jnp
from jax import lax
from jax.sharding import PartitionSpec as P

D = 4096
HEAD_DIM = 64
STATE = 128
CONV_WIDTH = 4
INNER = 4096
epsilon = 1e-06


def causal_conv(state_rows, newest, conv_weights):
    extended = jnp.concatenate([state_rows, newest[:, None]], axis=1)
    conv_sum = extended[:, 0] * conv_weights[0].astype(jnp.float32)
    for offset in range(1, conv_weights.shape[0]):
        conv_sum = conv_sum + extended[:, offset] * conv_weights[offset].astype(jnp.float32)
    return jax.nn.silu(conv_sum)


def product(left, right):
    return jnp.dot(left, right, preferred_element_type=jnp.float32)


def per_device(
    tokens,
    lengths,
    conv_state_x,
    conv_state_bc,
    ssm_state,
    norm_gain,
    w_gate,
    w_value,
    w_key,
    w_query,
    w_step,
    step_bias,
    decay_log,
    conv_x,
    conv_bc,
    inner_gain,
    w_out,
    mlp_gain,
    w_up,
    w_down,
):
    head_count = w_step.shape[1]
    group_count = w_key.shape[1] // STATE
    per_group = head_count // group_count
    widened = tokens.astype(jnp.float32)
    scaled = (widened * norm_gain.astype(jnp.float32)).astype(jnp.bfloat16)
    gate_raw, value_raw, key_raw, query_raw, step_raw, squares = (
        lax.psum_scatter(product(scaled, w_gate), "kv", scatter_dimension=0, tiled=True),
        lax.psum_scatter(product(scaled, w_value), "kv", scatter_dimension=0, tiled=True),
        lax.psum_scatter(product(scaled, w_key), "kv", scatter_dimension=0, tiled=True),
        lax.psum_scatter(product(scaled, w_query), "kv", scatter_dimension=0, tiled=True),
        lax.psum_scatter(product(scaled, w_step), "kv", scatter_dimension=0, tiled=True),
        lax.psum_scatter(jnp.sum(widened * widened, axis=1), "kv", scatter_dimension=0, tiled=True),
    )
    seq_count = gate_raw.shape[0]
    inverse = lax.rsqrt(squares / D + epsilon)[:, None]
    row_live = (
        jnp.arange(CONV_WIDTH - 1, dtype=jnp.int32)[None, :] >= CONV_WIDTH - 1 - lengths[:, None]
    ).astype(jnp.float32)
    live_x = conv_state_x.astype(jnp.float32) * row_live[:, :, None]
    live_bc = conv_state_bc.astype(jnp.float32) * row_live[:, :, None, None]
    mixed_values = causal_conv(live_x, value_raw * inverse, conv_x).reshape(
        seq_count, head_count, HEAD_DIM
    )
    key_query = causal_conv(
        live_bc, jnp.stack([key_raw * inverse, query_raw * inverse], axis=1), conv_bc
    )
    key_heads = jnp.repeat(
        key_query[:, 0].reshape(seq_count, group_count, STATE), per_group, axis=1
    )
    query_heads = jnp.repeat(
        key_query[:, 1].reshape(seq_count, group_count, STATE), per_group, axis=1
    )
    step_size = jax.nn.softplus(step_raw * inverse + step_bias)
    rate_now = -jnp.exp(decay_log) * step_size
    next_state = (
        ssm_state * jnp.exp(rate_now)[:, :, None, None]
        + (step_size[:, :, None] * mixed_values)[:, :, :, None] * key_heads[:, :, None, :]
    )
    mixer_y = jnp.einsum(
        "bhpn,bhn->bhp", next_state, query_heads, precision=lax.Precision.HIGHEST
    ).reshape(seq_count, head_count * HEAD_DIM)
    gated_rows = mixer_y * jax.nn.silu(gate_raw * inverse)
    gated_low = (gated_rows * inner_gain.astype(jnp.float32)).astype(jnp.bfloat16)
    all_low, all_squares = (
        lax.all_gather(gated_low, "kv", axis=0, tiled=True),
        lax.all_gather(
            jnp.sum(gated_rows * gated_rows, axis=1).astype(jnp.bfloat16), "kv", axis=0, tiled=True
        ).astype(jnp.float32),
    )
    out_sum, gated_total = lax.psum((product(all_low, w_out), all_squares), "tp")
    residual = (widened + out_sum * lax.rsqrt(gated_total / INNER + epsilon)[:, None]).astype(
        jnp.bfloat16
    )
    residual_wide = residual.astype(jnp.float32)
    hidden_low = (residual_wide * mlp_gain.astype(jnp.float32)).astype(jnp.bfloat16)
    row_squares = jnp.sum(residual_wide * residual_wide, axis=1)
    up_sum, square_sum = lax.psum((product(hidden_low, w_up), row_squares), "kv")
    activation = jnp.square(
        jax.nn.relu(up_sum * lax.rsqrt(square_sum / D + epsilon)[:, None])
    ).astype(jnp.bfloat16)
    down_sum = lax.psum(product(activation, w_down), "tp")
    layer_out = (residual_wide + down_sum).astype(jnp.bfloat16)
    return (layer_out, next_state)


def solution(mesh):
    return jax.shard_map(
        per_device,
        mesh=mesh,
        in_specs=(
            P("grp", "kv"),
            P(("grp", "kv")),
            P(("grp", "kv"), None, "tp"),
            P(("grp", "kv"), None, None, "tp"),
            P(("grp", "kv"), "tp", None, None),
            P("kv"),
            P("kv", "tp"),
            P("kv", "tp"),
            P("kv", "tp"),
            P("kv", "tp"),
            P("kv", "tp"),
            P("tp"),
            P("tp"),
            P(None, "tp"),
            P(None, None, "tp"),
            P("tp"),
            P("tp", "kv"),
            P("kv"),
            P("kv", "tp"),
            P("tp", "kv"),
        ),
        out_specs=(P("grp", "kv"), P(("grp", "kv"), "tp", None, None)),
        check_vma=False,
    )
```

profile of v0, /device:TPU:0, one launch (start us, length us, event | category | flops | bytes accessed | tf_op | source)
XLA Modules:
  0.0 207.7 jit_solution(14826090005879602014)
XLA Ops:
  7.2 0.0 copy-start
  7.2 0.0 copy-start.3
  7.2 0.0 all-reduce.20.cloned.1.call-start
  7.2 0.0 copy-start.2
  7.2 0.8 convert_element_type.73
  8.1 0.7 copy-done
  8.8 0.0 copy-start.4
  8.8 0.0 copy-start.5
  8.8 1.9 fusion.26
  10.7 0.0 copy-done.3
  10.7 0.0 copy-done.2
  10.7 0.0 copy-start.9
  10.7 0.0 copy-start.8
  10.7 0.0 copy-start.14
  10.7 1.0 fusion.20
  11.7 0.0 all-reduce.20.cloned.1.call-update
  11.8 0.0 all-reduce.14.cloned.1.call-start
  11.8 0.1 fusion.4
  12.0 0.0 copy-done.15
  12.0 0.0 copy-done.16
  12.0 0.0 copy-done.6
  12.0 0.1 fusion.28
  12.2 0.0 copy-done.4
  12.2 0.2 fusion.24
  12.3 0.2 fusion.22
  12.6 0.7 fusion.47
  13.9 21.3 %all-reduce.7 = (f32[16,256]{1,0:T(8,128)S(1)}, f32[16]{0:T(128)S(1)}, f32[16,256]{1,0:T(8,128)S(1)}, f32[16,16]{1,0:T(8,128)S(1)}) all-reduce(f32[16,256]{1,0:T(8,128)S(1)} %fusion.22, f32[16]{0:T(128)S(1)} %fusion.4, f32[16,256]{1,0:T(8,128)S(1)} %fusion.24, ...), channel_id=6, replica_groups=mesh['grp'=2,'kv'=4,'tp'=4] {'kv'}, use_global_device_ids=true, to_apply=%region_5.0.clone | all-reduce | flops 8464 | bytes 67712
  35.2 0.1 fusion.42
  35.3 0.1 convert_multiply_fusion.5
  35.4 0.1 fusion.38
  35.5 0.1 convert_multiply_fusion.4
  36.3 0.1 multiply_exponential_fusion
  36.4 13.2 %all-reduce.20.cloned.1.call-done = (f32[16,1024]{1,0:T(8,128)}, f32[16,1024]{1,0:T(8,128)}) async-done(((f32[16,1024]{1,0:T(8,128)}, f32[16,1024]{1,0:T(8,128)}), (f32[16,1024]{1,0:T(8,128)}, f32[16,1024]{1,0:T(8,128)})) %all-reduce.20.cloned.1.call-update) | async-done | bytes 131088
  49.5 0.8 divide_multiply_fusion.1
  50.4 0.1 reshape.72
  50.5 0.1 broadcast_multiply_fusion
  50.6 2.1 multiply_add_fusion
  52.6 0.0 copy-start.1
  52.6 0.0 copy-start.11
  52.6 0.0 copy-start.12
  52.7 1.3 copy-done.1
  53.9 3.3 %fusion.48 = f32[4,16,1,64]{3,2,1,0:T(1,128)S(1)} fusion(f32[4,16,64,128]{3,2,1,0:T(8,128)S(1)} %multiply_add_fusion, f32[4,16,128,1]{2,3,1,0:T(1,128)S(1)} %bitcast.104), kind=kOutput, calls=%fused_computation.85 | convolution fusion | flops 6291456 | bytes 2146304 | tf_op jit(solution)/shard_map/bhpn,bhn->bhp/dot_general | solution.py:86
  57.3 0.1 reshape.74
  57.4 1.0 multiply_reduce_fusion
  58.3 0.2 dynamic-update-slice
  58.6 0.0 copy-done.11
  58.6 10.6 %all-reduce = bf16[16]{0:T(256)(128)(2,1)S(1)} all-reduce(bf16[16]{0:T(256)(128)(2,1)S(1)} %dynamic-update-slice), channel_id=1, replica_groups=mesh['grp'=2,'kv'=4,'tp'=4] {'kv'}, use_global_device_ids=true, to_apply=%add | all-reduce | flops 16 | bytes 64
  69.2 0.0 copy-done.12
  69.2 5.7 %psum.36 = f32[16]{0:T(128)S(1)} all-reduce(bf16[16]{0:T(256)(128)(2,1)S(1)} %all-reduce), channel_id=1, replica_groups=mesh['grp'=2,'kv'=4,'tp'=4] {'tp'}, use_global_device_ids=true, to_apply=%region_9.10 | all-reduce | flops 16 | bytes 96 | tf_op jit(solution)/shard_map/psum | solution.py:97
  74.9 13.1 %all-gather = bf16[4,4,1024]{2,1,0:T(4,128)(2,1)S(1)} all-gather(bf16[1,4,1024]{2,1,0:T(4,128)(2,1)S(1)} %fusion.30), channel_id=1, replica_groups=mesh['grp'=2,'kv'=4,'tp'=4] {'kv'}, dimensions={0}, use_global_device_ids=true | all-gather | bytes 40960 | tf_op jit(solution)/shard_map/all_gather | solution.py:92
  88.0 2.6 %fusion.49 = f32[16,1024]{1,0:T(8,128)} fusion(bf16[16,1024]{1,0:T(8,128)(2,1)S(1)} %reshape.87, bf16[1024,1024]{1,0:T(8,128)(2,1)} %param.36), kind=kOutput, calls=%fused_computation.86 | convolution fusion | flops 33554432 | bytes 2195456 | tf_op jit(solution)/shard_map/dot_general | solution.py:23
  90.6 0.0 all-reduce.14.cloned.1.call-update
  90.7 0.0 all-reduce.16.cloned.1.call-start
  90.7 30.0 %all-reduce.14.cloned.1.call-done = f32[16,1024]{1,0:T(8,128)} async-done(((f32[16,1024]{1,0:T(8,128)}), f32[16,1024]{1,0:T(8,128)}) %all-reduce.14.cloned.1.call-update) | async-done | bytes 65552 | tf_op jit(solution)/shard_map/psum | solution.py:97
  120.7 1.0 fusion.7
  121.7 5.3 %fusion.9 = f32[16,4096]{1,0:T(8,128)} fusion(bf16[1024,4096]{1,0:T(8,128)(2,1)} %param.38, bf16[16,1024]{1,0:T(8,128)(2,1)S(1)} %get-tuple-element.9, f32[1024]{0:T(1024)S(1)} %convert_element_type.84), kind=kOutput, calls=%fused_computation.18 | convolution fusion | flops 134266880 | bytes 8687616 | tf_op jit(solution)/shard_map/dot_general | solution.py:23
  127.0 0.0 all-reduce.16.cloned.1.call-update
  127.0 0.0 all-reduce.18.cloned.1.call-start
  127.1 11.8 %psum.38 = f32[16]{0:T(128)S(1)} all-reduce(f32[16]{0:T(128)S(1)} %get-tuple-element.8), channel_id=1, replica_groups=mesh['grp'=2,'kv'=4,'tp'=4] {'kv'}, use_global_device_ids=true, to_apply=%region_12.13 | all-reduce | flops 16 | bytes 128 | tf_op jit(solution)/shard_map/psum | solution.py:104
  138.9 23.9 %all-reduce.16.cloned.1.call-done = f32[16,4096]{1,0:T(8,128)} async-done(((f32[16,4096]{1,0:T(8,128)}), f32[16,4096]{1,0:T(8,128)}) %all-reduce.16.cloned.1.call-update) | async-done | bytes 262160 | tf_op jit(solution)/shard_map/psum | solution.py:104
  162.8 5.3 %fusion = f32[16,1024]{1,0:T(8,128)} fusion(bf16[4096,1024]{1,0:T(8,128)(2,1)} %param.39, f32[16,4096]{1,0:T(8,128)} %all-reduce.16.cloned.1.call-done, f32[16]{0:T(128)S(1)} %add_rsqrt_fusion), kind=kOutput, calls=%fused_computation.2 | convolution fusion | flops 134479872 | bytes 8716352 | tf_op jit(solution)/shard_map/dot_general | solution.py:23
  168.1 0.0 all-reduce.18.cloned.1.call-update
  168.2 31.6 %all-reduce.18.cloned.1.call-done = f32[16,1024]{1,0:T(8,128)} async-done(((f32[16,1024]{1,0:T(8,128)}), f32[16,1024]{1,0:T(8,128)}) %all-reduce.18.cloned.1.call-update) | async-done | bytes 65552 | tf_op jit(solution)/shard_map/psum | solution.py:108
  199.7 1.5 fusion.8
  (31 shorter events, 0.2 us)
Async XLA Ops:
  7.2 1.6 copy-start
  7.2 3.5 %copy-start.3 = (bf16[16,1024]{1,0:T(8,128)(2,1)S(1)}, bf16[16,1024]{1,0:T(8,128)(2,1)}, u32[]{:S(2)}) copy-start(bf16[16,1024]{1,0:T(8,128)(2,1)} %param.20) | copy-start | bytes 98308
  7.2 42.3 %all-reduce.20.cloned.1.call-start = ((), (), s32[]{:S(2)}) async-start(), calls=%async_computation.3 | async-start | bytes 262144
  7.2 3.4 %copy-start.2 = (bf16[1024,1024]{1,0:T(8,128)(2,1)S(1)}, bf16[1024,1024]{1,0:T(8,128)(2,1)}, u32[]{:S(2)}) copy-start(bf16[1024,1024]{1,0:T(8,128)(2,1)} %param.26) | copy-start | bytes 6291460
  8.8 3.2 %copy-start.15 = (s32[4]{0:T(128)S(1)}, s32[4]{0:T(128)}, u32[]{:S(2)}) copy-start(s32[4]{0:T(128)} %param.21) | copy-start | bytes 52
  8.8 3.2 %copy-start.16 = (f32[16]{0:T(128)S(1)}, f32[16]{0:T(128)}, u32[]{:S(2)}) copy-start(f32[16]{0:T(128)} %param.32) | copy-start | bytes 196
  8.8 3.2 %copy-start.6 = (bf16[1024,16]{0,1:T(8,128)(2,1)S(1)}, bf16[1024,16]{0,1:T(8,128)(2,1)}, u32[]{:S(2)}) copy-start(bf16[1024,16]{0,1:T(8,128)(2,1)} %param.30) | copy-start | bytes 98308
  8.8 3.4 %copy-start.10 = (bf16[4,2,256]{2,1,0:T(2,128)(2,1)S(1)}, bf16[4,2,256]{2,1,0:T(2,128)(2,1)}, u32[]{:S(2)}) copy-start(bf16[4,2,256]{2,1,0:T(2,128)(2,1)} %param.34) | copy-start | bytes 12292
  8.8 3.4 %copy-start.4 = (bf16[1024,256]{1,0:T(8,128)(2,1)S(1)}, bf16[1024,256]{1,0:T(8,128)(2,1)}, u32[]{:S(2)}) copy-start(bf16[1024,256]{1,0:T(8,128)(2,1)} %param.28) | copy-start | bytes 1572868
  8.8 3.5 %copy-start.5 = (bf16[1024,256]{1,0:T(8,128)(2,1)S(1)}, bf16[1024,256]{1,0:T(8,128)(2,1)}, u32[]{:S(2)}) copy-start(bf16[1024,256]{1,0:T(8,128)(2,1)} %param.29) | copy-start | bytes 1572868
  10.7 1.8 copy-start.7
  10.7 1.9 copy-start.13
  10.7 24.6 %copy-start.9 = (bf16[4,3,2,256]{3,2,1,0:T(2,128)(2,1)S(1)}, bf16[4,3,2,256]{3,2,1,0:T(2,128)(2,1)}, u32[]{:S(2)}) copy-start(bf16[4,3,2,256]{3,2,1,0:T(2,128)(2,1)} %param.23) | copy-start | bytes 36868
  10.7 24.8 %copy-start.8 = (bf16[4,3,1024]{2,0,1:T(4,128)(2,1)S(1)}, bf16[4,3,1024]{2,0,1:T(4,128)(2,1)}, u32[]{:S(2)}) copy-start(bf16[4,3,1024]{2,0,1:T(4,128)(2,1)} %param.22) | copy-start | bytes 73732
  10.7 25.6 %copy-start.14 = (f32[16]{0:T(128)S(1)}, f32[16]{0:T(128)}, u32[]{:S(2)}) copy-start(f32[16]{0:T(128)} %param.31) | copy-start | bytes 196
  11.8 108.9 %all-reduce.14.cloned.1.call-start = ((), (), s32[]{:S(2)}) async-start(), calls=%async_computation | async-start | bytes 131072 | tf_op jit(solution)/shard_map/psum | solution.py:97
  52.6 1.3 copy-start.1
  52.6 6.0 %copy-start.11 = (bf16[1024]{0:T(1024)(128)(2,1)S(1)}, bf16[1024]{0:T(1024)(128)(2,1)}, u32[]{:S(2)}) copy-start(bf16[1024]{0:T(1024)(128)(2,1)} %param.35) | copy-start | bytes 6148
  52.6 16.6 %copy-start.12 = (bf16[1024]{0:T(1024)(128)(2,1)S(1)}, bf16[1024]{0:T(1024)(128)(2,1)}, u32[]{:S(2)}) copy-start(bf16[1024]{0:T(1024)(128)(2,1)} %param.37) | copy-start | bytes 6148
  90.7 72.2 %all-reduce.16.cloned.1.call-start = ((), (), s32[]{:S(2)}) async-start(), calls=%async_computation.1 | async-start | bytes 524288 | tf_op jit(solution)/shard_map/psum | solution.py:104
  127.0 72.7 %all-reduce.18.cloned.1.call-start = ((), (), s32[]{:S(2)}) async-start(), calls=%async_computation.2 | async-start | bytes 131072 | tf_op jit(solution)/shard_map/psum | solution.py:108
Sparse Core Ops, SparseCore 0:
  11.9 37.6 all-reduce.19
  90.8 29.8 all-reduce.13
  127.2 35.5 all-reduce.15
  168.3 31.3 all-reduce.17
where the time goes:
time: 208 us
  waiting for transfers between devices  98.7 us (47%)
  blocking collectives  62.5 us (30%)
  matrix products  19.9 us (10%)
  between operations  15.4 us (7%)
  other arithmetic  7.87 us (4%)
  local copies, waits for them, and re-layouts  3.2 us (2%)
    unnamed x2, blocking collectives  31.9 us
    psum x1, waiting for transfers between devices, per_device(): down_sum = lax.psum(product(activation, w_down), 'tp')  31.6 us
    psum x1, waiting for transfers between devices, per_device(): lax.psum((product(all_low, w_out), all_squares), 'tp')  30 us
    psum x1, waiting for transfers between devices, per_device(): lax.psum((product(hidden_low, w_up), row_squares), 'kv')  23.9 us
    dot_general x8, matrix products, product(): return jnp.dot(left, right, preferred_element_type=jnp.float32)  16.6 us
    unnamed x5, waiting for transfers between devices  13.2 us
    all_gather x1, blocking collectives, per_device(): lax.all_gather(gated_low, 'kv', axis=0, tiled=True)  13.1 us
    psum x1, blocking collectives, per_device(): lax.psum((product(hidden_low, w_up), row_squares), 'kv')  11.8 us
  transfers between devices with their start and end apart: 4, of which 4 were waited for; matrix products, arithmetic and copies ran while one was open for 1% of the time, Pallas kernels for 0%

commit v1 on v0

--- a/solution.py
+++ b/solution.py
@@ -105,7 +105,7 @@
     activation = jnp.square(
         jax.nn.relu(up_sum * lax.rsqrt(square_sum / D + epsilon)[:, None])
     ).astype(jnp.bfloat16)
-    down_sum = lax.psum(product(activation, w_down), "tp")
+    down_sum = jnp.sum(lax.all_gather(product(activation, w_down), "tp"), axis=0)
     layer_out = (residual_wide + down_sum).astype(jnp.bfloat16)
     return (layer_out, next_state)
 

time: 208 us -> 181 us (0.87)
  waiting for transfers between devices: 98.7 us -> 67.2 us
  blocking collectives: 62.5 us -> 68.3 us
    psum x1 -> x0, waiting for transfers between devices: 31.6 us -> none  [per_device(): down_sum = lax.psum(product(activation, w_down), 'tp')]
    all_gather x0 -> x1, blocking collectives: none -> 5.77 us  [per_device(): lax.all_gather(product(activation, w_down), 'tp')]
    unnamed x5 -> x4, waiting for transfers between devices: 13.2 us -> 13.3 us
  transfers between devices with their start and end apart: 4 -> 3, of which waited for: 4 -> 3; matrix products, arithmetic and copies ran while one was open for 1% -> 1% of each run, Pallas kernels for 0% -> 0%
where the time goes in v1:
time: 181 us; the launch traced here: 180 us
  blocking collectives  68.3 us (38%)
  waiting for transfers between devices  67.2 us (37%)
  matrix products  19.3 us (11%)
  between operations  15.3 us (8%)
  other arithmetic  7.05 us (4%)
  local copies, waits for them, and re-layouts  3.15 us (2%)
    unnamed x2, blocking collectives  31.9 us
    psum x1, waiting for transfers between devices, per_device(): lax.psum((product(all_low, w_out), all_squares), 'tp')  30 us
    psum x1, waiting for transfers between devices, per_device(): lax.psum((product(hidden_low, w_up), row_squares), 'kv')  24 us
    dot_general x8, matrix products, product(): return jnp.dot(left, right, preferred_element_type=jnp.float32)  16 us
    unnamed x4, waiting for transfers between devices  13.3 us
    all_gather x1, blocking collectives, per_device(): lax.all_gather(gated_low, 'kv', axis=0, tiled=True)  13.1 us
    psum x1, blocking collectives, per_device(): lax.psum((product(hidden_low, w_up), row_squares), 'kv')  11.8 us
    all_gather x1, blocking collectives, per_device(): lax.all_gather(product(activation, w_down), 'tp')  5.77 us
  transfers between devices with their start and end apart: 3, of which 3 were waited for; matrix products, arithmetic and copies ran while one was open for 1% of the time, Pallas kernels for 0%

profile of v1, /device:TPU:0, one launch (start us, length us, event | category | flops | bytes accessed | tf_op | source)
XLA Modules:
  0.0 180.5 jit_solution(1329660261869002265)
XLA Ops:
  7.2 0.0 copy-start
  7.2 0.0 copy-start.3
  7.2 0.0 all-reduce.17.cloned.1.call-start
  7.2 0.0 copy-start.2
  7.2 0.8 convert_element_type.73
  8.1 0.7 copy-done
  8.8 0.0 copy-start.4
  8.8 0.0 copy-start.5
  8.8 1.9 %fusion.26 = f32[16,1024]{1,0:T(8,128)} fusion(bf16[1024,1024]{1,0:T(8,128)(2,1)S(1)} %copy-done, bf16[16,1024]{1,0:T(8,128)(2,1)} %param.20, f32[1024]{0:T(1024)S(1)} %convert_element_type.73), kind=kOutput, calls=%fused_computation.43 | convolution fusion | flops 33603584 | bytes 2199552 | tf_op jit(solution)/shard_map/dot_general | solution.py:23
  10.7 0.0 copy-done.3
  10.7 0.0 copy-done.2
  10.7 0.0 copy-start.9
  10.7 0.0 copy-start.8
  10.7 0.0 copy-start.14
  10.7 1.0 fusion.20
  11.8 0.0 all-reduce.17.cloned.1.call-update
  11.8 0.0 all-reduce.13.cloned.1.call-start
  11.8 0.1 fusion.4
  12.0 0.0 copy-done.15
  12.0 0.0 copy-done.16
  12.0 0.0 copy-done.6
  12.0 0.1 fusion.28
  12.2 0.0 copy-done.10
  12.2 0.0 copy-done.4
  12.2 0.2 fusion.24
  12.4 0.0 copy-done.5
  12.4 0.2 fusion.22
  12.5 0.0 copy-done.7
  12.6 0.0 copy-done.13
  12.6 0.6 fusion.47
  13.9 21.3 %all-reduce.7 = (f32[16,256]{1,0:T(8,128)S(1)}, f32[16]{0:T(128)S(1)}, f32[16,256]{1,0:T(8,128)S(1)}, f32[16,16]{1,0:T(8,128)S(1)}) all-reduce(f32[16,256]{1,0:T(8,128)S(1)} %fusion.22, f32[16]{0:T(128)S(1)} %fusion.4, f32[16,256]{1,0:T(8,128)S(1)} %fusion.24, ...), channel_id=7, replica_groups=mesh['grp'=2,'kv'=4,'tp'=4] {'kv'}, use_global_device_ids=true, to_apply=%region_5.0.clone | all-reduce | flops 8464 | bytes 67712
  35.1 0.1 fusion.42
  35.2 0.1 convert_multiply_fusion.5
  35.3 0.1 fusion.38
  35.5 0.1 convert_multiply_fusion.4
  36.2 0.1 multiply_exponential_fusion
  36.3 13.2 %all-reduce.17.cloned.1.call-done = (f32[16,1024]{1,0:T(8,128)}, f32[16,1024]{1,0:T(8,128)}) async-done(((f32[16,1024]{1,0:T(8,128)}, f32[16,1024]{1,0:T(8,128)}), (f32[16,1024]{1,0:T(8,128)}, f32[16,1024]{1,0:T(8,128)})) %all-reduce.17.cloned.1.call-update) | async-done | bytes 131088
  49.5 0.8 divide_multiply_fusion.1
  50.4 0.1 reshape.72
  50.5 0.1 broadcast_multiply_fusion
  50.5 2.1 %multiply_add_fusion = f32[4,16,64,128]{3,2,1,0:T(8,128)S(1)} fusion(f32[4,16,64,128]{3,2,1,0:T(8,128)} %param.24, f32[4,16,128]{2,1,0:T(8,128)S(1)} %broadcast_bitcast_fusion, f32[4,16,64]{2,1,0:T(8,128)S(1)} %broadcast_multiply_fusion, f32[4,16]{1,0:T(4,128)S(1)} %get-tuple-element.12), kind=kLoop, calls=%fused_computation | loop fusion | flops 1572864 | bytes 4243712 | tf_op jit(solution)/shard_map/add | solution.py:83
  52.6 0.0 copy-start.1
  52.6 0.0 copy-start.11
  52.6 0.0 copy-start.12
  52.6 1.3 copy-done.1
  53.9 3.3 %fusion.48 = f32[4,16,1,64]{3,2,1,0:T(1,128)S(1)} fusion(f32[4,16,64,128]{3,2,1,0:T(8,128)S(1)} %multiply_add_fusion, f32[4,16,128,1]{2,3,1,0:T(1,128)S(1)} %bitcast.106), kind=kOutput, calls=%fused_computation.85 | convolution fusion | flops 6291456 | bytes 2146304 | tf_op jit(solution)/shard_map/bhpn,bhn->bhp/dot_general | solution.py:86
  57.3 0.1 reshape.74
  57.4 1.0 multiply_reduce_fusion
  58.3 0.2 dynamic-update-slice
  58.6 10.6 %all-reduce = bf16[16]{0:T(256)(128)(2,1)S(1)} all-reduce(bf16[16]{0:T(256)(128)(2,1)S(1)} %dynamic-update-slice), channel_id=1, replica_groups=mesh['grp'=2,'kv'=4,'tp'=4] {'kv'}, use_global_device_ids=true, to_apply=%add | all-reduce | flops 16 | bytes 64
  69.2 5.7 %psum.29 = f32[16]{0:T(128)S(1)} all-reduce(bf16[16]{0:T(256)(128)(2,1)S(1)} %all-reduce), channel_id=1, replica_groups=mesh['grp'=2,'kv'=4,'tp'=4] {'tp'}, use_global_device_ids=true, to_apply=%region_9.10 | all-reduce | flops 16 | bytes 96 | tf_op jit(solution)/shard_map/psum | solution.py:97
  74.9 13.1 %all-gather.1 = bf16[4,4,1024]{2,1,0:T(4,128)(2,1)S(1)} all-gather(bf16[1,4,1024]{2,1,0:T(4,128)(2,1)S(1)} %fusion.30), channel_id=1, replica_groups=mesh['grp'=2,'kv'=4,'tp'=4] {'kv'}, dimensions={0}, use_global_device_ids=true | all-gather | bytes 40960 | tf_op jit(solution)/shard_map/all_gather | solution.py:92
  88.0 2.6 %fusion.49 = f32[16,1024]{1,0:T(8,128)} fusion(bf16[16,1024]{1,0:T(8,128)(2,1)S(1)} %reshape.88, bf16[1024,1024]{1,0:T(8,128)(2,1)} %param.36), kind=kOutput, calls=%fused_computation.86 | convolution fusion | flops 33554432 | bytes 2195456 | tf_op jit(solution)/shard_map/dot_general | solution.py:23
  90.6 0.0 all-reduce.13.cloned.1.call-update
  90.7 0.0 all-reduce.15.cloned.1.call-start
  90.7 30.0 %all-reduce.13.cloned.1.call-done = f32[16,1024]{1,0:T(8,128)} async-done(((f32[16,1024]{1,0:T(8,128)}), f32[16,1024]{1,0:T(8,128)}) %all-reduce.13.cloned.1.call-update) | async-done | bytes 65552 | tf_op jit(solution)/shard_map/psum | solution.py:97
  120.7 1.0 fusion.7
  121.7 5.3 %fusion.9 = f32[16,4096]{1,0:T(8,128)} fusion(bf16[1024,4096]{1,0:T(8,128)(2,1)} %param.38, bf16[16,1024]{1,0:T(8,128)(2,1)S(1)} %get-tuple-element.9, f32[1024]{0:T(1024)S(1)} %convert_element_type.84), kind=kOutput, calls=%fused_computation.18 | convolution fusion | flops 134266880 | bytes 8687616 | tf_op jit(solution)/shard_map/dot_general | solution.py:23
  127.0 0.0 all-reduce.15.cloned.1.call-update
  127.1 11.8 %psum.31 = f32[16]{0:T(128)S(1)} all-reduce(f32[16]{0:T(128)S(1)} %get-tuple-element.8), channel_id=1, replica_groups=mesh['grp'=2,'kv'=4,'tp'=4] {'kv'}, use_global_device_ids=true, to_apply=%region_12.13 | all-reduce | flops 16 | bytes 128 | tf_op jit(solution)/shard_map/psum | solution.py:104
  138.9 24.0 %all-reduce.15.cloned.1.call-done = f32[16,4096]{1,0:T(8,128)} async-done(((f32[16,4096]{1,0:T(8,128)}), f32[16,4096]{1,0:T(8,128)}) %all-reduce.15.cloned.1.call-update) | async-done | bytes 262160 | tf_op jit(solution)/shard_map/psum | solution.py:104
  162.8 4.7 %fusion = f32[16,1024]{1,0:T(8,128)S(1)} fusion(bf16[4096,1024]{1,0:T(8,128)(2,1)} %param.39, f32[16,4096]{1,0:T(8,128)} %all-reduce.15.cloned.1.call-done, f32[16]{0:T(128)S(1)} %add_rsqrt_fusion), kind=kOutput, calls=%fused_computation.2 | convolution fusion | flops 134479872 | bytes 8716352 | tf_op jit(solution)/shard_map/dot_general | solution.py:23
  167.5 5.8 %all-gather = f32[64,1024]{1,0:T(8,128)S(1)} all-gather(f32[16,1024]{1,0:T(8,128)S(1)} %fusion), channel_id=2, replica_groups=mesh['grp'=2,'kv'=4,'tp'=4] {'tp'}, dimensions={0}, use_global_device_ids=true | all-gather | bytes 327680 | tf_op jit(solution)/shard_map/all_gather | solution.py:108
  173.3 0.6 fusion.8
  (30 shorter events, 0.2 us)
Async XLA Ops:
  7.2 1.6 copy-start
  7.2 3.5 %copy-start.3 = (bf16[16,1024]{1,0:T(8,128)(2,1)S(1)}, bf16[16,1024]{1,0:T(8,128)(2,1)}, u32[]{:S(2)}) copy-start(bf16[16,1024]{1,0:T(8,128)(2,1)} %param.20) | copy-start | bytes 98308
  7.2 42.3 %all-reduce.17.cloned.1.call-start = ((), (), s32[]{:S(2)}) async-start(), calls=%async_computation.2 | async-start | bytes 262144
  7.2 3.4 %copy-start.2 = (bf16[1024,1024]{1,0:T(8,128)(2,1)S(1)}, bf16[1024,1024]{1,0:T(8,128)(2,1)}, u32[]{:S(2)}) copy-start(bf16[1024,1024]{1,0:T(8,128)(2,1)} %param.26) | copy-start | bytes 6291460
  8.8 3.2 %copy-start.15 = (s32[4]{0:T(128)S(1)}, s32[4]{0:T(128)}, u32[]{:S(2)}) copy-start(s32[4]{0:T(128)} %param.21) | copy-start | bytes 52
  8.8 3.2 %copy-start.16 = (f32[16]{0:T(128)S(1)}, f32[16]{0:T(128)}, u32[]{:S(2)}) copy-start(f32[16]{0:T(128)} %param.32) | copy-start | bytes 196
  8.8 3.2 %copy-start.6 = (bf16[1024,16]{0,1:T(8,128)(2,1)S(1)}, bf16[1024,16]{0,1:T(8,128)(2,1)}, u32[]{:S(2)}) copy-start(bf16[1024,16]{0,1:T(8,128)(2,1)} %param.30) | copy-start | bytes 98308
  8.8 3.4 %copy-start.10 = (bf16[4,2,256]{2,1,0:T(2,128)(2,1)S(1)}, bf16[4,2,256]{2,1,0:T(2,128)(2,1)}, u32[]{:S(2)}) copy-start(bf16[4,2,256]{2,1,0:T(2,128)(2,1)} %param.34) | copy-start | bytes 12292
  8.8 3.4 %copy-start.4 = (bf16[1024,256]{1,0:T(8,128)(2,1)S(1)}, bf16[1024,256]{1,0:T(8,128)(2,1)}, u32[]{:S(2)}) copy-start(bf16[1024,256]{1,0:T(8,128)(2,1)} %param.28) | copy-start | bytes 1572868
  8.8 3.6 %copy-start.5 = (bf16[1024,256]{1,0:T(8,128)(2,1)S(1)}, bf16[1024,256]{1,0:T(8,128)(2,1)}, u32[]{:S(2)}) copy-start(bf16[1024,256]{1,0:T(8,128)(2,1)} %param.29) | copy-start | bytes 1572868
  10.7 1.9 %copy-start.7 = (bf16[4,1024]{1,0:T(4,128)(2,1)S(1)}, bf16[4,1024]{1,0:T(4,128)(2,1)}, u32[]{:S(2)}) copy-start(bf16[4,1024]{1,0:T(4,128)(2,1)} %param.33) | copy-start | bytes 24580
  10.7 1.9 %copy-start.13 = (u32[32]{0:T(128)S(1)}, u32[32]{0:T(128)}, u32[]{:S(2)}) copy-start(u32[32]{0:T(128)} %constant.29) | copy-start | bytes 388
  10.7 24.5 %copy-start.9 = (bf16[4,3,2,256]{3,2,1,0:T(2,128)(2,1)S(1)}, bf16[4,3,2,256]{3,2,1,0:T(2,128)(2,1)}, u32[]{:S(2)}) copy-start(bf16[4,3,2,256]{3,2,1,0:T(2,128)(2,1)} %param.23) | copy-start | bytes 36868
  10.7 24.8 %copy-start.8 = (bf16[4,3,1024]{2,0,1:T(4,128)(2,1)S(1)}, bf16[4,3,1024]{2,0,1:T(4,128)(2,1)}, u32[]{:S(2)}) copy-start(bf16[4,3,1024]{2,0,1:T(4,128)(2,1)} %param.22) | copy-start | bytes 73732
  10.7 25.5 %copy-start.14 = (f32[16]{0:T(128)S(1)}, f32[16]{0:T(128)}, u32[]{:S(2)}) copy-start(f32[16]{0:T(128)} %param.31) | copy-start | bytes 196
  11.8 108.9 %all-reduce.13.cloned.1.call-start = ((), (), s32[]{:S(2)}) async-start(), calls=%async_computation | async-start | bytes 131072 | tf_op jit(solution)/shard_map/psum | solution.py:97
  52.6 1.3 copy-start.1
  52.6 6.0 %copy-start.11 = (bf16[1024]{0:T(1024)(128)(2,1)S(1)}, bf16[1024]{0:T(1024)(128)(2,1)}, u32[]{:S(2)}) copy-start(bf16[1024]{0:T(1024)(128)(2,1)} %param.35) | copy-start | bytes 6148
  52.6 16.6 %copy-start.12 = (bf16[1024]{0:T(1024)(128)(2,1)S(1)}, bf16[1024]{0:T(1024)(128)(2,1)}, u32[]{:S(2)}) copy-start(bf16[1024]{0:T(1024)(128)(2,1)} %param.37) | copy-start | bytes 6148
  90.7 72.2 %all-reduce.15.cloned.1.call-start = ((), (), s32[]{:S(2)}) async-start(), calls=%async_computation.1 | async-start | bytes 524288 | tf_op jit(solution)/shard_map/psum | solution.py:104
Sparse Core Ops, SparseCore 0:
  11.9 37.5 all-reduce.16
  90.8 29.8 all-reduce.12
  127.2 35.5 all-reduce.14
